TPU v7x, 32 devices: a whole 2x2x4 slice. The times are simulated.
32 devices in a mesh: ep: 16 (over z, y, x), tp: 2 (over core).
Axes of the slice: x: 2, y: 2, z: 4, core: 2. Of those that a mesh axis runs over, the one named last changes fastest.
Arguments:
- tokens: bfloat16 [256, 2048], P('ep'), may hold values from -6 to 6
- lengths: int32 [256], P('ep'), may hold values from 1 to 1024
- gain_first: float32 [2048], replicated, may hold values from 0.1 to 1.9
- w_query: bfloat16 [2048, 1024], P(None, 'tp'), may hold values from -0.125 to 0.125
- w_key: bfloat16 [2048, 256], P(None, 'tp'), may hold values from -0.125 to 0.125
- w_value: bfloat16 [2048, 256], P(None, 'tp'), may hold values from -0.125 to 0.125
- cache_keys: bfloat16 [256, 1024, 256], P('ep', None, 'tp'), may hold values from -400 to 400
- cache_values: bfloat16 [256, 1024, 256], P('ep', None, 'tp'), may hold values from -6 to 6
- lambdas: float32 [8], P('tp'), may hold values from 0.3 to 0.8
- head_gain: float32 [8, 128], P('tp'), may hold values from 0.1 to 1.9
- w_output: bfloat16 [1024, 2048], replicated, may hold values from -0.1875 to 0.1875
- gain_second: float32 [2048], replicated, may hold values from 0.1 to 1.9
- w_group: bfloat16 [2048, 4], replicated, may hold values from -0.125 to 0.125
- w_router: bfloat16 [2048, 16], replicated, may hold values from -0.125 to 0.125
- w_blend: bfloat16 [2048], replicated, may hold values from -0.125 to 0.125
- routes: int32 [256, 4], P('ep'), may hold values from 0 to 15, all different within a row; in each aligned block of 16 rows (0 to 15, 16 to 31, ...) at most 8 rows name the same one
- w_expert_gate: bfloat16 [16, 2048, 512], P('ep', None, 'tp'), may hold values from -0.125 to 0.125
- w_expert_up: bfloat16 [16, 2048, 512], P('ep', None, 'tp'), may hold values from -0.125 to 0.125
- w_expert_down: bfloat16 [16, 512, 2048], P('ep', 'tp'), may hold values from -0.25 to 0.25
- w_dense_gate: bfloat16 [2048, 4096], P(None, ('ep', 'tp')), may hold values from -0.125 to 0.125
- w_dense_up: bfloat16 [2048, 4096], P(None, ('ep', 'tp')), may hold values from -0.125 to 0.125
- w_dense_down: bfloat16 [4096, 2048], P(('ep', 'tp')), may hold values from -0.1875 to 0.1875
Outputs:
- layer_out: bfloat16 [256, 2048], P('ep', 'tp')
Inputs may be any that keep to these rules, and one draw needn't show every extreme that they name: `routes`: in the rows of one index of ep no expert is named by more than 8 rows, a bound that some block reaches; a row names 4 different experts.
All inputs are finite; a program needn't handle non-finite values.
Results may differ from a plain program's by a relative error of at most 0.012.
The roundings to bfloat16 on the way count: a program that leaves them out, or rounds other values in their place, can miss the bound.
Values may be sent and summed in bfloat16 or wider, within the bound.
A program may use at most 128 MiB of HBM per device.

v0:
```python
import jax
import jax.numpy as jnp
from jax import lax
from jax.sharding import PartitionSpec as P

HD = 64
VD = 128
N_GROUPS = 4


def layer_norm(values, gain):
    floats = values.astype(jnp.float32)
    center = floats - jnp.mean(floats, -1, keepdims=True)
    spread = jnp.mean(center * center, -1, keepdims=True)
    return center * lax.rsqrt(spread + 1e-05) * gain


def rotate(values, position):
    half = values.shape[-1] // 2
    inverse = 10000.0 ** (-jnp.arange(half, dtype=jnp.float32) / half)
    angle = position.astype(jnp.float32)[..., None] * inverse
    cosine = jnp.cos(angle)
    sine = jnp.sin(angle)
    first = values[..., :half]
    second = values[..., half:]
    return jnp.concatenate([first * cosine - second * sine, second * cosine + first * sine], -1)


def local(
    tokens,
    lengths,
    gain_first,
    w_query,
    w_key,
    w_value,
    cache_keys,
    cache_values,
    lambdas,
    head_gain,
    w_output,
    gain_second,
    w_group,
    w_router,
    w_blend,
    routes,
    w_expert_gate,
    w_expert_up,
    w_expert_down,
    w_dense_gate,
    w_dense_up,
    w_dense_down,
):
    seqs, width = tokens.shape
    ep_count = lax.axis_size("ep")
    tp_count = lax.axis_size("tp")
    heads_here = lambdas.shape[0]
    kv_here = w_key.shape[1] // (2 * HD)
    group = heads_here // kv_here
    scale = HD ** (-0.5)
    normed = layer_norm(tokens, gain_first).astype(jnp.bfloat16)
    query = jnp.dot(normed, w_query, preferred_element_type=jnp.float32).reshape(
        seqs, kv_here, group, 2, HD
    )
    query = rotate(query, lengths[:, None, None, None]).astype(jnp.bfloat16)
    key_new = jnp.dot(normed, w_key, preferred_element_type=jnp.float32).reshape(
        seqs, kv_here, 2, HD
    )
    key_new = rotate(key_new, lengths[:, None, None]).astype(jnp.bfloat16)
    value_new = jnp.dot(normed, w_value, preferred_element_type=jnp.float32).astype(jnp.bfloat16)
    value_new = value_new.reshape(seqs, kv_here, VD)
    keys = cache_keys.reshape(seqs, -1, kv_here, 2, HD)
    values = cache_values.reshape(seqs, -1, kv_here, VD)
    span = keys.shape[1]
    scores = (
        jnp.einsum("skgcd,slkcd->skgcl", query, keys, preferred_element_type=jnp.float32) * scale
    )
    valid = jnp.arange(span)[None, :] < lengths[:, None]
    scores = jnp.where(valid[:, None, None, None, :], scores, -jnp.inf)
    own = jnp.einsum("skgcd,skcd->skgc", query, key_new, preferred_element_type=jnp.float32) * scale
    top = jnp.maximum(jnp.max(scores, -1), own)
    expo = jnp.exp(scores - top[..., None])
    own_e = jnp.exp(own - top)
    total = jnp.sum(expo, -1) + own_e
    probs = expo / total[..., None]
    own_p = own_e / total
    lam = lambdas.reshape(kv_here, group)
    weights = (probs[:, :, :, 0] - lam[None, :, :, None] * probs[:, :, :, 1]).astype(jnp.bfloat16)
    own_w = (own_p[..., 0] - lam[None] * own_p[..., 1]).astype(jnp.bfloat16)
    mixed = jnp.einsum("skgl,slkv->skgv", weights, values, preferred_element_type=jnp.float32)
    mixed = (
        mixed + own_w.astype(jnp.float32)[..., None] * value_new.astype(jnp.float32)[:, :, None, :]
    )
    mixed = mixed.reshape(seqs, heads_here, VD)
    heads = mixed * lax.rsqrt(jnp.mean(mixed * mixed, -1, keepdims=True) + 1e-05) * head_gain
    heads = heads.astype(jnp.bfloat16).reshape(seqs, heads_here * VD)
    all_heads = lax.all_gather(heads, "tp", axis=1, tiled=True)
    resid = tokens.astype(jnp.float32) + jnp.dot(
        all_heads, w_output, preferred_element_type=jnp.float32
    )
    moe_in = layer_norm(resid, gain_second).astype(jnp.bfloat16)
    experts = w_router.shape[1]
    per_group = experts // N_GROUPS
    top_k = routes.shape[1]
    group_probs = jax.nn.softmax(jnp.dot(moe_in, w_group, preferred_element_type=jnp.float32), -1)
    expert_logits = jnp.dot(moe_in, w_router, preferred_element_type=jnp.float32)
    onehot = (routes[:, :, None] == jnp.arange(experts, dtype=jnp.int32)[None, None, :]).astype(
        jnp.float32
    )
    group_hot = (
        (routes // per_group)[:, :, None] == jnp.arange(N_GROUPS, dtype=jnp.int32)[None, None, :]
    ).astype(jnp.float32)
    chosen = jnp.sum(onehot * expert_logits[:, None, :], -1)
    group_part = jnp.sum(group_hot * group_probs[:, None, :], -1)
    route_weight = (group_part * jax.nn.softmax(chosen, -1)).astype(jnp.bfloat16)
    table = jnp.sum(onehot * route_weight.astype(jnp.float32)[:, :, None], 1).astype(jnp.bfloat16)
    blend = jax.nn.sigmoid(jnp.dot(moe_in, w_blend, preferred_element_type=jnp.float32)).astype(
        jnp.bfloat16
    )
    rows_all, table_all, blend_all = (
        lax.all_gather(moe_in, "ep", axis=0, tiled=True),
        lax.all_gather(table, "ep", axis=0, tiled=True),
        lax.all_gather(blend, "ep", axis=0, tiled=True),
    )
    dense_gate = jnp.dot(rows_all, w_dense_gate, preferred_element_type=jnp.float32)
    dense_up = jnp.dot(rows_all, w_dense_up, preferred_element_type=jnp.float32)
    dense_hidden = (
        blend_all.astype(jnp.float32)[:, None] * jax.nn.silu(dense_gate) * dense_up
    ).astype(jnp.bfloat16)
    capacity = 2 * seqs * top_k // experts
    column = lax.dynamic_slice_in_dim(table_all, lax.axis_index("ep"), 1, 1)[:, 0].astype(
        jnp.float32
    )
    column = column.reshape(ep_count, seqs)
    hit_count = (column > 0.0).astype(jnp.int32)
    ranks = jnp.cumsum(hit_count, 1) - 1
    slot_mask = (ranks[:, None, :] == jnp.arange(capacity, dtype=jnp.int32)[None, :, None]) & (
        hit_count[:, None, :] > 0
    )
    slot_pick = slot_mask.astype(jnp.bfloat16)
    slot_float = slot_mask.astype(jnp.float32)
    picked = (
        jnp.einsum(
            "bcs,bsd->bcd",
            slot_pick,
            rows_all.reshape(ep_count, seqs, width),
            preferred_element_type=jnp.float32,
        )
        .astype(jnp.bfloat16)
        .reshape(ep_count * capacity, width)
    )
    slot_weight = jnp.einsum("bcs,bs->bc", slot_float, column, precision=lax.Precision.HIGHEST)
    expert_hidden = (
        jax.nn.silu(jnp.dot(picked, w_expert_gate[0], preferred_element_type=jnp.float32))
        * jnp.dot(picked, w_expert_up[0], preferred_element_type=jnp.float32)
    ).astype(jnp.bfloat16)
    half = width // tp_count
    own_half = lax.dynamic_slice_in_dim(resid, lax.axis_index("tp") * half, half, 1)
    hidden_both, expert_both = (
        lax.all_gather(dense_hidden, "tp", axis=1, tiled=True),
        lax.all_gather(expert_hidden, "tp", axis=1, tiled=True),
    )
    dense_rows, expert_rows = (
        lax.all_to_all(w_dense_down, "tp", split_axis=1, concat_axis=0, tiled=True),
        lax.all_to_all(w_expert_down[0], "tp", split_axis=1, concat_axis=0, tiled=True),
    )
    dense_term = jnp.einsum(
        "bsf,fd->bsd",
        hidden_both.reshape(ep_count, seqs, -1),
        dense_rows,
        preferred_element_type=jnp.float32,
    )
    expert_out = jnp.dot(expert_both, expert_rows, preferred_element_type=jnp.float32)
    expert_out = expert_out * slot_weight.reshape(-1)[:, None]
    back = jnp.einsum(
        "bcs,bcd->bsd",
        slot_float,
        expert_out.reshape(ep_count, capacity, half),
        precision=lax.Precision.HIGHEST,
    )
    term = (dense_term + back).reshape(ep_count * seqs, half)
    summed = lax.psum_scatter(term, "ep", scatter_dimension=0, tiled=True)
    return (own_half + summed).astype(jnp.bfloat16)


def solution(mesh):
    return jax.shard_map(
        local,
        mesh=mesh,
        in_specs=(
            P("ep", None),
            P("ep"),
            P(),
            P(None, "tp"),
            P(None, "tp"),
            P(None, "tp"),
            P("ep", None, "tp"),
            P("ep", None, "tp"),
            P("tp"),
            P("tp", None),
            P(),
            P(),
            P(),
            P(),
            P(),
            P("ep", None),
            P("ep", None, "tp"),
            P("ep", None, "tp"),
            P("ep", "tp", None),
            P(None, ("ep", "tp")),
            P(None, ("ep", "tp")),
            P(("ep", "tp"), None),
        ),
        out_specs=P("ep", "tp"),
        check_vma=False,
    )
```

profile of v0, /device:TPU:0, one launch (start us, length us, event | category | flops | bytes accessed | tf_op | source)
XLA Modules:
  0.0 224.9 jit_solution(6640174355717355612)
XLA Ops:
  6.6 0.8 convert_element_type.116
  7.4 0.7 iota_compare_fusion.1
  8.1 1.0 convert_reduce_fusion
  9.1 1.0 fusion.23
  10.1 1.3 fusion.64
  11.6 1.3 fusion.66
  12.8 0.1 reshape.391
  12.9 0.1 fusion.68
  13.1 0.1 multiply_cosine_fusion
  13.4 0.2 fusion.43
  13.7 6.4 %copy.90 = bf16[16,1024,128]{1,2,0:T(8,128)(2,1)} copy(bf16[16,1024,128]{2,1,0:T(8,128)(2,1)} %param.28) | data formatting | bytes 8388608 | tf_op args[6]
  20.2 3.0 %fusion.69 = (f32[16,4,2]{1,2,0:T(2,128)S(1)}, f32[16,1,4,2,1024]{4,2,3,0,1:T(4,128)S(1)}) fusion(bf16[16,1024,2,64]{1,3,2,0:T(8,128)(2,1)} %bitcast.167, bf16[16,4,2,32]{3,1,2,0:T(4,128)(2,1)S(1)} %get-tuple-element.6, bf16[16,4,2,32]{3,1,2,0:T(4,128)(2,1)S(1)} %get-tuple-element.5, pred[16,1024]{1,0:T(8,128)(4,1)S(1)} %iota_compare_fusion.1), kind=kOutput, calls=%fused_computation.122 | convolution fusion | flops 17203072 | bytes 4751872 | tf_op jit(solution)/shard_map/skgcd,slkcd->skgcl/dot_general | solution.py:75
  23.4 0.3 fusion.17
  24.0 0.3 fusion.16
  24.4 1.4 fusion.7
  25.9 3.0 %multiply_reduce_fusion.1 = (f32[16,4]{1,0:T(8,128)S(1)}, f32[16,4,128]{2,1,0:T(4,128)S(1)}) fusion(f32[16,128]{1,0:T(8,128)S(1)} %fusion.7, f32[16,4]{1,0:T(8,128)S(1)} %copy.96, bf16[16,1024,128]{2,1,0:T(8,128)(2,1)} %param.29, f32[16,1,4,2,1024]{4,2,3,0,1:T(4,128)S(1)} %fusion.16, f32[4]{0:T(128)S(1)} %copy-done.13), kind=kOutput, calls=%fused_computation.63 | convolution fusion | flops 17006528 | bytes 4760080 | tf_op jit(solution)/shard_map/skgl,slkv->skgv/dot_general | solution.py:89
  29.0 2.1 all_gather.18
  31.1 0.8 fusion.70
  31.9 0.2 multiply_reduce_fusion
  32.1 0.7 multiply_convert_fusion
  32.9 1.3 copy.98
  34.2 3.6 %all-to-all-start.1 = ((bf16[256,2,1024]{0,2,1:T(8,128)(2,1)}), bf16[256,2,1024]{0,2,1:T(8,128)(2,1)S(1)}, u32[]{:S(2)}, u32[]{:S(2)}) async-start(bf16[256,2,1024]{0,2,1:T(8,128)(2,1)} %bitcast.171), calls=%async_computation.1 | async-start | bytes 2097152 | tf_op jit(solution)/shard_map/all_to_all | solution.py:164
  37.8 0.2 fusion.73
  38.0 0.2 fusion.71
  38.1 0.2 select_reduce_fusion.1
  38.5 42.8 %all_gather.22 = bf16[256,16]{1,0:T(8,128)(2,1)S(1)} all-gather(bf16[16,16]{1,0:T(8,128)(2,1)S(1)} %select_reduce_fusion), channel_id=1, replica_groups=mesh['ep'=16,'tp'=2] {'ep'}, dimensions={0}, use_global_device_ids=true | all-gather | bytes 8704 | tf_op jit(solution)/shard_map/all_gather | solution.py:121
  81.4 0.2 dynamic-slice_reduce_fusion
  81.8 0.6 dynamic-slice
  83.0 0.1 fusion.12
  83.1 0.2 dynamic-update-slice
  83.4 36.6 %all-reduce = bf16[256]{0:T(256)(128)(2,1)S(1)} all-reduce(bf16[256]{0:T(256)(128)(2,1)S(1)} %dynamic-update-slice), channel_id=1, replica_groups=mesh['ep'=16,'tp'=2] {'ep'}, use_global_device_ids=true, to_apply=%add | all-reduce | flops 256 | bytes 1024
  120.0 0.2 reduce_window_sum.11
  120.2 0.1 fusion.31
  120.4 1.9 copy.125
  122.3 4.2 %all-to-all-start = ((bf16[128,2,1024]{2,0,1:T(8,128)(2,1)}), bf16[128,2,1024]{2,0,1:T(8,128)(2,1)}, u32[]{:S(2)}, u32[]{:S(2)}) async-start(bf16[128,2,1024]{2,0,1:T(8,128)(2,1)} %bitcast.173), calls=%async_computation | async-start | bytes 1048576 | tf_op jit(solution)/shard_map/all_to_all | solution.py:163
  126.6 1.5 copy.99
  128.1 1.9 fusion.72
  130.1 1.8 fusion.5
  131.9 2.0 all_gather.21
  133.9 0.3 fusion
  134.2 0.3 fusion.14
  134.5 0.3 fusion.6
  134.8 1.9 all_gather.23
  136.7 0.3 fusion.1
  137.0 0.7 fusion.29
  137.7 2.3 %convolution_add_fusion.1 = f32[16,16,1024]{2,1,0:T(8,128)} fusion(f32[16,16,1024]{2,1,0:T(8,128)S(1)} %fusion.29, bf16[16,16,256]{2,1,0:T(8,128)(2,1)S(1)} %bitcast.175, bf16[256,1024,1]{1,0,2:T(8,128)(2,1)} %bitcast.26), kind=kOutput, calls=%fused_computation.3 | convolution fusion | flops 134479872 | bytes 2752512 | tf_op jit(solution)/shard_map/bsf,fd->bsd/dot_general | solution.py:166
  140.1 76.6 %reduce-scatter.2.cloned.1.call-done = f32[16,1024]{1,0:T(8,128)} async-done(((f32[256,1024]{1,0:T(8,128)}), f32[16,1024]{1,0:T(8,128)}) %reduce-scatter.2.cloned.1.call-update) | async-done | bytes 65552 | tf_op jit(solution)/shard_map/reduce_scatter | solution.py:181
  216.6 1.5 add_convert_fusion
  (80 shorter events, 1.8 us)
Async XLA Ops:
  6.5 5.0 %copy-start = (bf16[2048,512]{1,0:T(8,128)(2,1)S(1)}, bf16[2048,512]{1,0:T(8,128)(2,1)}, u32[]{:S(2)}) copy-start(bf16[2048,512]{1,0:T(8,128)(2,1)} %param.25) | copy-start | bytes 6291460
  6.5 121.5 %all-gather.2.cloned.1.call-start = ((), (), s32[]{:S(2)}) async-start(), calls=%async_computation.3 | async-start | bytes 1114112 | tf_op jit(solution)/shard_map/all_gather | solution.py:120
  20.2 4.1 %copy-start.13 = (f32[4]{0:T(128)S(1)}, f32[4]{0:T(128)}, u32[]{:S(2)}) copy-start(f32[4]{0:T(128)} %param.30) | copy-start | bytes 52
  20.2 4.3 %copy-start.4 = (bf16[16,2048]{1,0:T(8,128)(2,1)S(1)}, bf16[16,2048]{1,0:T(8,128)(2,1)}, u32[]{:S(2)}) copy-start(bf16[16,2048]{1,0:T(8,128)(2,1)} %param.22) | copy-start | bytes 196612
  20.2 4.3 %copy-start.10 = (f32[2048]{0:T(1024)S(1)}, f32[2048]{0:T(1024)}, u32[]{:S(2)}) copy-start(f32[2048]{0:T(1024)} %param.24) | copy-start | bytes 24580
  23.2 5.8 %copy-start.14 = (f32[4,128]{1,0:T(4,128)S(1)}, f32[4,128]{1,0:T(4,128)}, u32[]{:S(2)}) copy-start(f32[4,128]{1,0:T(4,128)} %param.31) | copy-start | bytes 6148
  24.4 6.7 %copy-start.1 = (bf16[1024,2048]{1,0:T(8,128)(2,1)S(1)}, bf16[1024,2048]{1,0:T(8,128)(2,1)}, u32[]{:S(2)}) copy-start(bf16[1024,2048]{1,0:T(8,128)(2,1)} %param.32) | copy-start | bytes 12582916
  25.9 6.3 %copy-start.11 = (f32[2048]{0:T(1024)S(1)}, f32[2048]{0:T(1024)}, u32[]{:S(2)}) copy-start(f32[2048]{0:T(1024)} %param.33) | copy-start | bytes 24580
  28.8 4.0 %copy-start.5 = (bf16[1,256,2048]{2,1,0:T(8,128)(2,1)S(1)}, bf16[1,256,2048]{2,1,0:T(8,128)(2,1)}, u32[]{:S(2)}) copy-start(bf16[1,256,2048]{2,1,0:T(8,128)(2,1)} %param.40) | copy-start | bytes 3145732
  31.1 6.7 %copy-start.8 = (bf16[2048,16]{0,1:T(8,128)(2,1)S(1)}, bf16[2048,16]{0,1:T(8,128)(2,1)}, u32[]{:S(2)}) copy-start(bf16[2048,16]{0,1:T(8,128)(2,1)} %param.35) | copy-start | bytes 196612
  31.1 6.9 %copy-start.16 = (bf16[2048,4]{0,1:T(4,128)(2,1)S(1)}, bf16[2048,4]{0,1:T(4,128)(2,1)}, u32[]{:S(2)}) copy-start(bf16[2048,4]{0,1:T(4,128)(2,1)} %param.34) | copy-start | bytes 49156
  31.1 7.0 %copy-start.9 = (s32[16,4]{0,1:T(4,128)S(1)}, s32[16,4]{0,1:T(4,128)}, u32[]{:S(2)}) copy-start(s32[16,4]{0,1:T(4,128)} %param.37) | copy-start | bytes 772
  31.1 50.6 %copy-start.12 = (bf16[2048]{0:T(1024)(128)(2,1)S(1)}, bf16[2048]{0:T(1024)(128)(2,1)}, u32[]{:S(2)}) copy-start(bf16[2048]{0:T(1024)(128)(2,1)} %param.36) | copy-start | bytes 12292
  31.1 50.6 %copy-start.17 = (u32[32]{0:T(128)S(1)}, u32[32]{0:T(128)}, u32[]{:S(2)}) copy-start(u32[32]{0:T(128)} %constant.77) | copy-start | bytes 388
  32.8 5.0 %copy-start.7 = (bf16[16,2048]{1,0:T(8,128)(2,1)S(1)}, bf16[16,2048]{1,0:T(8,128)(2,1)}, u32[]{:S(2)}) copy-start(bf16[16,2048]{1,0:T(8,128)(2,1)} %multiply_convert_fusion) | copy-start | bytes 196612
  34.2 88.1 %all-to-all-start.1 = ((bf16[256,2,1024]{0,2,1:T(8,128)(2,1)}), bf16[256,2,1024]{0,2,1:T(8,128)(2,1)S(1)}, u32[]{:S(2)}, u32[]{:S(2)}) async-start(bf16[256,2,1024]{0,2,1:T(8,128)(2,1)} %bitcast.171), calls=%async_computation.1 | async-start | bytes 2097152 | tf_op jit(solution)/shard_map/all_to_all | solution.py:164
  122.3 4.3 %copy-start.3 = (bf16[256,2,1024]{0,2,1:T(8,128)(2,1)}, bf16[256,2,1024]{0,2,1:T(8,128)(2,1)S(1)}, u32[]{:S(2)}) copy-start(bf16[256,2,1024]{0,2,1:T(8,128)(2,1)S(1)} %all-to-all-done.1) | copy-start | bytes 3145732
  122.3 15.4 %all-to-all-start = ((bf16[128,2,1024]{2,0,1:T(8,128)(2,1)}), bf16[128,2,1024]{2,0,1:T(8,128)(2,1)}, u32[]{:S(2)}, u32[]{:S(2)}) async-start(bf16[128,2,1024]{2,0,1:T(8,128)(2,1)} %bitcast.173), calls=%async_computation | async-start | bytes 1048576 | tf_op jit(solution)/shard_map/all_to_all | solution.py:163
  126.5 90.1 %reduce-scatter.2.cloned.1.call-start = ((), (), s32[]{:S(2)}) async-start(), calls=%async_computation.4 | async-start | bytes 1114112 | tf_op jit(solution)/shard_map/reduce_scatter | solution.py:181
  128.1 5.8 %copy-start.2 = (bf16[256,2048]{1,0:T(8,128)(2,1)S(1)}, bf16[256,2048]{1,0:T(8,128)(2,1)}, u32[]{:S(2)}) copy-start(bf16[256,2048]{1,0:T(8,128)(2,1)} %all-gather.2.cloned.1.call-done) | copy-start | bytes 3145732
  128.1 6.0 %copy-start.6 = (bf16[1,2048,256]{2,1,0:T(8,128)(2,1)S(1)}, bf16[1,2048,256]{2,1,0:T(8,128)(2,1)}, u32[]{:S(2)}) copy-start(bf16[1,2048,256]{2,1,0:T(8,128)(2,1)} %param.38) | copy-start | bytes 3145732
  128.1 6.4 %copy-start.15 = (bf16[1,2048,256]{2,1,0:T(8,128)(2,1)S(1)}, bf16[1,2048,256]{2,1,0:T(8,128)(2,1)}, u32[]{:S(2)}) copy-start(bf16[1,2048,256]{2,1,0:T(8,128)(2,1)} %param.39) | copy-start | bytes 3145732
Sparse Core Ops, SparseCore 0:
  33.0 58.0 all-gather.1
  140.2 76.4 reduce-scatter.1
where the time goes:
time: 226 us; the launch traced here: 225 us
  blocking collectives  85.4 us (38%)
  waiting for transfers between devices  76.6 us (34%)
  matrix products  19.6 us (9%)
  between operations  14.5 us (6%)
  local copies, waits for them, and re-layouts  13.4 us (6%)
  starting transfers between devices  7.83 us (3%)
  other arithmetic  7.67 us (3%)
    reduce_scatter x1, waiting for transfers between devices, local(): summed = lax.psum_scatter(term, 'ep', scatter_dimension=0, tiled=True)  76.6 us
    all_gather x1, blocking collectives, local(): lax.all_gather(table, 'ep', axis=0, tiled=True)  42.8 us
    unnamed x1, blocking collectives  36.6 us
    unnamed x42, local copies, waits for them, and re-layouts  8.69 us
  transfers between devices with their start and end apart: 4, of which 1 were waited for; matrix products, arithmetic and copies ran while one was open for 6% of the time, Pallas kernels for 0%

commit v1 on v0

v1 whole, which is shorter than its diff:
```python
import functools

import jax
import jax.numpy as jnp
from jax import lax
from jax.experimental import pallas as pl
from jax.experimental.pallas import tpu as pltpu
from jax.sharding import PartitionSpec as P

HD = 64
VD = 128
N_GROUPS = 4


def norm(floats, gain):
    center = floats - jnp.mean(floats, -1, keepdims=True)
    spread = jnp.mean(center * center, -1, keepdims=True)
    return center * lax.rsqrt(spread + 1e-05) * gain


MESH = pl.DeviceIdType.MESH
BF16 = jnp.bfloat16
F32 = jnp.float32


def layer_kernel(
    n,
    experts,
    lengths,
    lambdas,
    tokens,
    trig,
    gain_first,
    head_gain,
    gain_second,
    routes,
    w_small,
    wq_hbm,
    wk_hbm,
    wv_hbm,
    keys_hbm,
    values_hbm,
    wo_hbm,
    wg_hbm,
    wu_hbm,
    wd_hbm,
    dg_hbm,
    du_hbm,
    dd_hbm,
    out,
    wqkv,
    keys,
    values,
    wo,
    q8,
    scores,
    mixed,
    heads,
    resid,
    buf,
    wgu,
    dgu,
    wd,
    dd,
    ehid,
    dhid,
    stage,
    mine,
    rbuf,
    local_sem,
    xs,
    xr,
    gs,
    gr,
    fs,
    fr,
    ws,
    wr,
    hs,
    hr,
    rs,
    rr,
):
    me = lax.axis_index("ep")
    core = lax.axis_index("tp")
    other = 1 - core
    seqs, width = tokens.shape
    half = width // 2
    ffe = wg_hbm.shape[2]
    ffd = dg_hbm.shape[1]
    group = head_gain.shape[0]
    span = keys.shape[1]
    partner = (me, other)

    local = []

    def fetch(src, dst):
        copy = pltpu.make_async_copy(src, dst, local_sem.at[len(local)])
        copy.start()
        local.append(copy)

    qw, kw, vw = wq_hbm.shape[1], wk_hbm.shape[1], wv_hbm.shape[1]
    fetch(wq_hbm, wqkv.at[:, pl.ds(0, qw)])
    fetch(wk_hbm, wqkv.at[:, pl.ds(qw, kw)])
    fetch(wv_hbm, wqkv.at[:, pl.ds(qw + kw, vw)])
    parts = 4
    step = seqs // parts
    for p in range(parts):
        fetch(keys_hbm.at[pl.ds(p * step, step)], keys.at[pl.ds(p * step, step)])

    barrier = pltpu.get_barrier_semaphore()

    def greet(d, carry):
        pl.semaphore_signal(
            barrier, inc=1, device_id=(lax.rem(me + d, n), core), device_id_type=MESH
        )
        return carry

    pl.semaphore_signal(barrier, inc=1, device_id=partner, device_id_type=MESH)
    lax.fori_loop(1, n, greet, 0)

    floats = tokens[...].astype(F32)
    normed = norm(floats, gain_first[...]).astype(BF16)
    for copy in local[:3]:
        copy.wait()
    for p in range(parts):
        fetch(values_hbm.at[pl.ds(p * step, step)], values.at[pl.ds(p * step, step)])
    fetch(wo_hbm, wo)
    fetch(dg_hbm, dgu.at[:, pl.ds(0, ffd)])
    fetch(du_hbm, dgu.at[:, pl.ds(ffd, ffd)])
    fetch(wg_hbm.at[0], wgu.at[:, pl.ds(0, ffe)])
    fetch(wu_hbm.at[0], wgu.at[:, pl.ds(ffe, ffe)])
    mine_cols = pl.ds(pl.multiple_of(core * half, 128), half)
    fetch(wd_hbm.at[0, :, mine_cols], wd.at[0])
    fetch(dd_hbm.at[:, mine_cols], dd.at[0])
    proj = jnp.dot(normed, wqkv[...], preferred_element_type=F32)
    cosine, sine = trig[0], trig[1]
    lane = lax.broadcasted_iota(jnp.int32, cosine.shape, 1)
    upper = lane % HD >= HD // 2

    def rotated(x):
        swapped = jnp.where(upper, pltpu.roll(x, HD // 2, 1), pltpu.roll(x, 2 * HD - HD // 2, 1))
        return (x * cosine + swapped * sine).astype(BF16).astype(F32)

    for g in range(group):
        query = rotated(proj[:, g * 2 * HD : (g + 1) * 2 * HD])
        for c in range(2):
            q8[:, c * group + g, :] = jnp.where(lane // HD == c, query, 0.0)
    key_new = rotated(proj[:, qw : qw + kw])
    value_new = proj[:, qw + kw :].astype(BF16).astype(F32)

    pl.semaphore_wait(barrier, n)
    their_cols = pl.ds(pl.multiple_of(other * half, 128), half)
    give_wd = pltpu.make_async_remote_copy(
        src_ref=wd_hbm.at[0, :, their_cols],
        dst_ref=wd.at[1],
        send_sem=ws.at[0],
        recv_sem=wr.at[0],
        device_id=partner,
        device_id_type=MESH,
    )
    give_wd.start()
    give_dd = pltpu.make_async_remote_copy(
        src_ref=dd_hbm.at[:, their_cols],
        dst_ref=dd.at[1],
        send_sem=ws.at[1],
        recv_sem=wr.at[1],
        device_id=partner,
        device_id_type=MESH,
    )
    give_dd.start()

    scale = HD ** (-0.5)
    place = lax.broadcasted_iota(jnp.int32, (2 * group, span), 1)
    for p in range(parts):
        local[3 + p].wait()
        for s in range(p * step, (p + 1) * step):
            score = lax.dot_general(
                q8[s].astype(BF16),
                keys[s],
                (((1,), (1,)), ((), ())),
                preferred_element_type=F32,
            )
            scores[s] = jnp.where(place < lengths[s], score * scale, -jnp.inf)
    row = lax.broadcasted_iota(jnp.int32, (2 * group, 1), 0)
    lam = jnp.zeros((2 * group, 1), F32)
    for g in range(group):
        lam = jnp.where(row == g, lambdas[g], lam)
    gain = jnp.concatenate([head_gain[...], head_gain[...]], 0)
    for p in range(parts):
        at = slice(p * step, (p + 1) * step)
        own = jnp.sum(q8[at] * key_new[at][:, None, :], -1, keepdims=True) * scale
        score = scores[at]
        top = jnp.maximum(jnp.max(score, -1, keepdims=True), own)
        expo = jnp.exp(score - top)
        own_e = jnp.exp(own - top)
        total = 1.0 / (jnp.sum(expo, -1, keepdims=True) + own_e)
        probs = expo * total
        own_p = own_e * total
        flipped = jnp.concatenate([probs[:, group:], probs[:, :group]], 1)
        own_flipped = jnp.concatenate([own_p[:, group:], own_p[:, :group]], 1)
        weights = (probs - lam[None] * flipped).astype(BF16)
        own_w = (own_p - lam[None] * own_flipped).astype(BF16).astype(F32)
        local[3 + parts + p].wait()
        for s in range(step):
            mixed[p * step + s] = jnp.dot(
                weights[s], values[p * step + s], preferred_element_type=F32
            )
        mix = mixed[at] + own_w * value_new[at][:, None, :]
        square = jnp.mean(mix * mix, -1, keepdims=True)
        mixed[at] = mix * lax.rsqrt(square + 1e-05) * gain[None]
    for g in range(group):
        heads[core, :, g * VD : (g + 1) * VD] = mixed[:, g, :].astype(BF16)
    swap = pltpu.make_async_remote_copy(
        src_ref=heads.at[core],
        dst_ref=heads.at[core],
        send_sem=xs.at[0],
        recv_sem=xr.at[0],
        device_id=partner,
        device_id_type=MESH,
    )
    swap.start()
    local[3 + 2 * parts].wait()
    deep = group * VD
    after = floats + jnp.dot(
        heads[core],
        wo[pl.ds(pl.multiple_of(core * deep, deep), deep)],
        preferred_element_type=F32,
    )
    swap.wait_recv()
    after += jnp.dot(
        heads[other],
        wo[pl.ds(pl.multiple_of(other * deep, deep), deep)],
        preferred_element_type=F32,
    )
    resid[...] = after
    moe_in = norm(after, gain_second[...]).astype(BF16)
    logits = jnp.dot(moe_in, w_small[...], preferred_element_type=F32)
    spot = lax.broadcasted_iota(jnp.int32, logits.shape, 1)
    hit = spot == routes[:, 0:1]
    for k in range(1, routes.shape[1]):
        hit = hit | (spot == routes[:, k : k + 1])
    chosen = jnp.where(hit, logits, -jnp.inf)
    chosen = jnp.exp(chosen - jnp.max(chosen, -1, keepdims=True))
    chosen = chosen / jnp.sum(chosen, -1, keepdims=True)
    grouped = (spot >= experts) & (spot < experts + N_GROUPS)
    groups = jnp.where(grouped, logits, -jnp.inf)
    groups = jnp.exp(groups - jnp.max(groups, -1, keepdims=True))
    groups = groups / jnp.sum(groups, -1, keepdims=True)
    per_group = experts // N_GROUPS
    part = jnp.zeros(logits.shape, F32)
    for g in range(N_GROUPS):
        one = jnp.sum(jnp.where(spot == experts + g, groups, 0.0), -1, keepdims=True)
        part = jnp.where(spot // per_group == g, one, part)
    blend_here = jnp.where(spot == experts + N_GROUPS, jax.nn.sigmoid(logits), 0.0)
    extra_here = jnp.where(hit, part * chosen, blend_here).astype(BF16)
    for h in range(2):
        buf[me, h, :, :half] = moe_in[:, h * half : (h + 1) * half]
        buf[me, h, :, half:] = extra_here

    def gather_copy(d):
        return pltpu.make_async_remote_copy(
            src_ref=buf.at[me, core],
            dst_ref=buf.at[me, core],
            send_sem=gs.at[d],
            recv_sem=gr.at[d],
            device_id=(lax.rem(me + d, n), core),
            device_id_type=MESH,
        )

    def gather_start(d, carry):
        gather_copy(d).start()
        return carry

    lax.fori_loop(1, n, gather_start, 0)

    def forward_copy(d):
        source = lax.rem(me - d + n, n)
        return pltpu.make_async_remote_copy(
            src_ref=buf.at[source, core],
            dst_ref=buf.at[source, core],
            send_sem=fs.at[d],
            recv_sem=fr.at[d],
            device_id=partner,
            device_id_type=MESH,
        )

    def forward(d, carry):
        gather_copy(d).wait_recv()
        forward_copy(d).start()
        return carry

    lax.fori_loop(1, n, forward, 0)

    def forward_done(d, carry):
        forward_copy(d).wait_recv()
        return carry

    lax.fori_loop(1, n, forward_done, 0)
    for copy in local[4 + 2 * parts :]:
        copy.wait()

    blocks = min(n, max(1, 256 // seqs))
    rows = blocks * seqs

    def weights_of(j):
        extra = buf[pl.ds(j * blocks, blocks), 0, :, half:].reshape(rows, -1).astype(F32)
        lane = lax.broadcasted_iota(jnp.int32, extra.shape, 1)
        column = jnp.sum(jnp.where(lane == me, extra, 0.0), -1, keepdims=True)
        blend = jnp.sum(jnp.where(lane == experts + N_GROUPS, extra, 0.0), -1, keepdims=True)
        return column, blend

    def up(j, carry):
        _, blend = weights_of(j)
        at = pl.ds(pl.multiple_of(j * rows, rows), rows)
        dense = jnp.zeros((rows, 2 * ffd), F32)
        expert = jnp.zeros((rows, 2 * ffe), F32)
        for h in range(width // half):
            x = buf[pl.ds(j * blocks, blocks), h, :, :half].reshape(rows, half)
            dense += jnp.dot(x, dgu[h * half : (h + 1) * half], preferred_element_type=F32)
            expert += jnp.dot(x, wgu[h * half : (h + 1) * half], preferred_element_type=F32)
        dhid[0, at] = (blend * jax.nn.silu(dense[:, :ffd]) * dense[:, ffd:]).astype(BF16)
        ehid[0, at] = (jax.nn.silu(expert[:, :ffe]) * expert[:, ffe:]).astype(BF16)
        return carry

    lax.fori_loop(0, n // blocks, up, 0)

    give = []
    for k, hid in enumerate((dhid, ehid)):
        copy = pltpu.make_async_remote_copy(
            src_ref=hid.at[0],
            dst_ref=hid.at[1],
            send_sem=hs.at[k],
            recv_sem=hr.at[k],
            device_id=partner,
            device_id_type=MESH,
        )
        copy.start()
        give.append(copy)
    give_wd.wait_recv()
    give_dd.wait_recv()
    for copy in give:
        copy.wait_recv()

    def down(j, carry):
        column, _ = weights_of(j)
        at = pl.ds(pl.multiple_of(j * rows, rows), rows)
        expert = jnp.dot(ehid[0, at], wd[0], preferred_element_type=F32)
        expert += jnp.dot(ehid[1, at], wd[1], preferred_element_type=F32)
        dense = jnp.dot(dhid[0, at], dd[0], preferred_element_type=F32)
        dense += jnp.dot(dhid[1, at], dd[1], preferred_element_type=F32)
        term = dense + column * expert
        stage[pl.ds(j * blocks, blocks)] = term.reshape(blocks, seqs, half).astype(BF16)
        return carry

    lax.fori_loop(0, n // blocks, down, 0)

    def scatter_copy(d):
        target = lax.rem(me + d, n)
        return pltpu.make_async_remote_copy(
            src_ref=stage.at[target],
            dst_ref=rbuf.at[d],
            send_sem=rs.at[d],
            recv_sem=rr.at[d],
            device_id=(target, core),
            device_id_type=MESH,
        )

    def scatter_start(d, carry):
        scatter_copy(d).start()
        return carry

    lax.fori_loop(1, n, scatter_start, 0)
    mine[...] = resid[:, mine_cols] + stage[me].astype(F32)

    def collect(d, carry):
        scatter_copy(d).wait_recv()
        mine[...] += rbuf[d].astype(F32)
        return carry

    lax.fori_loop(1, n, collect, 0)
    out[...] = mine[...].astype(BF16)

    def drain(d, carry):
        gather_copy(d).wait_send()
        forward_copy(d).wait_send()
        scatter_copy(d).wait_send()
        return carry

    lax.fori_loop(1, n, drain, 0)
    swap.wait_send()
    give_wd.wait_send()
    give_dd.wait_send()
    for copy in give:
        copy.wait_send()


def local(
    tokens,
    lengths,
    gain_first,
    w_query,
    w_key,
    w_value,
    cache_keys,
    cache_values,
    lambdas,
    head_gain,
    w_output,
    gain_second,
    w_group,
    w_router,
    w_blend,
    routes,
    w_eg,
    w_eu,
    w_ed,
    w_dg,
    w_du,
    w_dd,
):
    n = lax.axis_size("ep")
    seqs, width = tokens.shape
    half = width // lax.axis_size("tp")
    span = cache_keys.shape[1]
    experts = w_router.shape[1]
    group = lambdas.shape[0]
    inverse = 10000.0 ** (-jnp.arange(HD // 2, dtype=F32) / (HD // 2))
    angle = lengths.astype(F32)[:, None] * inverse
    cosine, sine = jnp.cos(angle), jnp.sin(angle)
    trig = jnp.stack(
        [jnp.concatenate([cosine] * 4, 1), jnp.concatenate([-sine, sine, -sine, sine], 1)]
    )
    w_small = jnp.concatenate([w_router, w_group, w_blend[:, None]], 1)
    w_small = jnp.pad(w_small, ((0, 0), (0, -w_small.shape[1] % 128)))
    lanes = w_small.shape[1]
    spare = -w_dg.shape[1] % 128
    if spare:
        w_dg = jnp.pad(w_dg, ((0, 0), (0, spare)))
        w_du = jnp.pad(w_du, ((0, 0), (0, spare)))
        w_dd = jnp.pad(w_dd, ((0, spare), (0, 0)))
    ffe, ffd = w_eg.shape[2], w_dg.shape[1]
    dma = pltpu.SemaphoreType.DMA
    smem = pl.BlockSpec(memory_space=pltpu.SMEM)
    vmem = pl.BlockSpec(memory_space=pltpu.VMEM)
    anywhere = pl.BlockSpec(memory_space=pl.ANY)
    total = n * seqs
    columns = w_query.shape[1] + w_key.shape[1] + w_value.shape[1]
    return pl.pallas_call(
        functools.partial(layer_kernel, n, experts),
        out_shape=jax.ShapeDtypeStruct((seqs, half), BF16),
        in_specs=[smem] * 2 + [vmem] * 7 + [anywhere] * 12,
        out_specs=vmem,
        scratch_shapes=[
            pltpu.VMEM((width, columns), BF16),
            pltpu.VMEM(cache_keys.shape, BF16),
            pltpu.VMEM(cache_values.shape, BF16),
            pltpu.VMEM(w_output.shape, BF16),
            pltpu.VMEM((seqs, 2 * group, 2 * HD), F32),
            pltpu.VMEM((seqs, 2 * group, span), F32),
            pltpu.VMEM((seqs, 2 * group, VD), F32),
            pltpu.VMEM((2, seqs, group * VD), BF16),
            pltpu.VMEM((seqs, width), F32),
            pltpu.VMEM((n, 2, seqs, half + lanes), BF16),
            pltpu.VMEM((width, 2 * ffe), BF16),
            pltpu.VMEM((width, 2 * ffd), BF16),
            pltpu.VMEM((2, ffe, half), BF16),
            pltpu.VMEM((2, ffd, half), BF16),
            pltpu.VMEM((2, total, ffe), BF16),
            pltpu.VMEM((2, total, ffd), BF16),
            pltpu.VMEM((n, seqs, half), BF16),
            pltpu.VMEM((seqs, half), F32),
            pltpu.VMEM((n, seqs, half), BF16),
            dma((18,)),
            dma((1,)),
            dma((1,)),
            dma((n,)),
            dma((n,)),
            dma((n,)),
            dma((n,)),
            dma((2,)),
            dma((2,)),
            dma((2,)),
            dma((2,)),
            dma((n,)),
            dma((n,)),
        ],
        compiler_params=pltpu.CompilerParams(collective_id=0, has_side_effects=True),
        name="layer",
    )(
        lengths,
        lambdas,
        tokens,
        trig,
        gain_first.reshape(1, -1),
        head_gain,
        gain_second.reshape(1, -1),
        routes,
        w_small,
        w_query,
        w_key,
        w_value,
        cache_keys,
        cache_values,
        w_output,
        w_eg,
        w_eu,
        w_ed,
        w_dg,
        w_du,
        w_dd,
    )


def solution(mesh):
    return jax.shard_map(
        local,
        mesh=mesh,
        in_specs=(
            P("ep", None),
            P("ep"),
            P(),
            P(None, "tp"),
            P(None, "tp"),
            P(None, "tp"),
            P("ep", None, "tp"),
            P("ep", None, "tp"),
            P("tp"),
            P("tp", None),
            P(),
            P(),
            P(),
            P(),
            P(),
            P("ep", None),
            P("ep", None, "tp"),
            P("ep", None, "tp"),
            P("ep", "tp", None),
            P(None, ("ep", "tp")),
            P(None, ("ep", "tp")),
            P(("ep", "tp"), None),
        ),
        out_specs=P("ep", "tp"),
        check_vma=False,
    )
```

time: 226 us -> 51.6 us (0.23)
  the two profiles are of different devices: /device:TPU:0 before, /device:TPU:28 now
where the time goes in v1:
time: 51.6 us; the launch traced here: 51.3 us
  Pallas kernels  44.3 us (86%)
  local copies, waits for them, and re-layouts  4.61 us (9%)
  other arithmetic  2.36 us (5%)
    pallas_call x1, Pallas kernels, local(): pl.pallas_call(functools.partial(layer_kernel, n, experts), out_shape=jax...  44.3 us
    unnamed x2, local copies, waits for them, and re-layouts  2.73 us

profile of v1, /device:TPU:28, one launch (start us, length us, event | category | flops | bytes accessed | tf_op | source)
XLA Modules:
  0.0 51.3 jit_solution(13278900761880579969)
XLA Ops:
  0.0 0.7 %convert_element_type.5 = f32[16]{0:T(128)S(1)} convert(s32[16]{0:T(128)} %lengths.1) | non-fusion elementwise | flops 16 | bytes 128 | tf_op jit(solution)/shard_map/convert_element_type | solution.py:429
  0.7 0.1 multiply_cosine_fusion
  0.8 0.1 maximum_bitcast_fusion
  0.9 0.6 %pad_maximum_fusion.1.trig = f32[2,16,128]{2,1,0:T(8,128)} fusion(f32[1,16,128]{2,1,0:T(8,128)S(1)} %get-tuple-element.9, f32[1,16,128]{2,1,0:T(8,128)S(1)} %get-tuple-element.8), kind=kLoop, calls=%fused_computation.1 | loop fusion | flops 4096 | bytes 32768 | tf_op jit(solution)/shard_map/stack | solution.py:431
  1.5 0.7 %broadcast_in_dim.2 = bf16[2048,1]{0,1:T(2,128)(2,1)S(1)} reshape(bf16[2048]{0:T(1024)(128)(2,1)} %param.36) | data formatting | bytes 8192 | tf_op jit(solution)/shard_map/broadcast_in_dim | solution.py:434
  2.2 0.9 %pad_maximum_fusion = bf16[2048,21]{0,1:T(8,128)(2,1)S(1)} fusion(bf16[2048,1]{0,1:T(2,128)(2,1)S(1)} %broadcast_in_dim.2, bf16[2048,4]{0,1:T(4,128)(2,1)} %param.34, bf16[2048,16]{0,1:T(8,128)(2,1)} %param.35), kind=kLoop, calls=%fused_computation | loop fusion | flops 258048 | bytes 172032 | tf_op jit(solution)/shard_map/concatenate | solution.py:434
  3.1 0.3 copy.30
  3.4 0.9 %pad.4.w_small = bf16[2048,128]{1,0:T(8,128)(2,1)} pad(bf16[2048,21]{1,0:T(8,128)(2,1)S(1)} %copy.30, bf16[]{:T(256)} %constant.7.clone.1), padding=0_0x0_107 | pad | bytes 610306 | tf_op jit(solution)/shard_map/jit(_pad)/pad | solution.py:435
  4.3 1.4 %copy.31.routes = s32[16,4]{1,0:T(8,128)} copy(s32[16,4]{0,1:T(4,128)} %param.37) | data formatting | bytes 512 | tf_op args[15]
  5.6 44.3 %layer.1 = bf16[16,1024]{1,0:T(8,128)(2,1)} custom-call(s32[16]{0:T(128)} %lengths.1, f32[4]{0:T(128)} %lambdas.1, bf16[16,2048]{1,0:T(8,128)(2,1)} %tokens.1, f32[2,16,128]{2,1,0:T(8,128)} %pad_maximum_fusion.1.trig, f32[1,2048]{1,0:T(1,128)} %bitcast.6, f32[4,128]{1,0:T(4,128)} %head_gain.1, f32[1,2048]{1,0:T(1,128)} %bitcast.7, s32[16,4]{1,0:T(8,128)} %copy.31.routes, ...), custom_call_target="tpu_custom_call" | custom-call | tf_op jit(solution)/shard_map/layer/pallas_call | solution.py:449
  49.9 1.4 %copy.33 = bf16[16,1024]{1,0:T(8,128)(2,1)} copy(bf16[16,1024]{1,0:T(8,128)(2,1)} %layer.1) | data formatting | bytes 65536
  (1 shorter events, 0.0 us)

commit v2 on v1

--- a/solution.py
+++ b/solution.py
@@ -2,6 +2,7 @@
 
 import jax
 import jax.numpy as jnp
+import numpy as np
 from jax import lax
 from jax.experimental import pallas as pl
 from jax.experimental.pallas import tpu as pltpu
@@ -29,7 +30,7 @@
     lengths,
     lambdas,
     tokens,
-    trig,
+    inverse,
     gain_first,
     head_gain,
     gain_second,
@@ -66,10 +67,13 @@
     dhid,
     stage,
     mine,
-    rbuf,
+    near,
+    sums,
+    far,
     local_sem,
     xs,
     xr,
+    gz,
     gs,
     gr,
     fs,
@@ -80,6 +84,8 @@
     hr,
     rs,
     rr,
+    zs,
+    zr,
 ):
     me = lax.axis_index("ep")
     core = lax.axis_index("tp")
@@ -110,15 +116,37 @@
 
     barrier = pltpu.get_barrier_semaphore()
 
-    def greet(d, carry):
-        pl.semaphore_signal(
-            barrier, inc=1, device_id=(lax.rem(me + d, n), core), device_id_type=MESH
-        )
+    depth = 4 if n % 4 == 0 else 1
+    plane = n // depth
+    level, spot_here = me // plane, lax.rem(me, plane)
+
+    def level_mate(d):
+        return lax.rem(level + d, depth) * plane + spot_here
+
+    def plane_mate(d):
+        return level * plane + lax.rem(spot_here + d, plane)
+
+    def greet(target):
+        pl.semaphore_signal(barrier, inc=1, device_id=target, device_id_type=MESH)
+
+    def greet_plane(d, carry):
+        greet((plane_mate(d), core))
         return carry
 
-    pl.semaphore_signal(barrier, inc=1, device_id=partner, device_id_type=MESH)
-    lax.fori_loop(1, n, greet, 0)
-
+    greet(partner)
+    for d in range(1, depth):
+        greet((level_mate(d), core))
+    lax.fori_loop(1, plane, greet_plane, 0)
+
+    lane = lax.broadcasted_iota(jnp.int32, (seqs, 2 * HD), 1)
+    line = lax.broadcasted_iota(jnp.int32, (seqs, 2 * HD), 0)
+    upper = lane % HD >= HD // 2
+    position = jnp.zeros((seqs, 2 * HD), jnp.int32)
+    for s in range(seqs):
+        position = jnp.where(line == s, lengths[s], position)
+    angle = position.astype(F32) * inverse[...]
+    cosine = jnp.cos(angle)
+    sine = jnp.where(upper, jnp.sin(angle), -jnp.sin(angle))
     floats = tokens[...].astype(F32)
     normed = norm(floats, gain_first[...]).astype(BF16)
     for copy in local[:3]:
@@ -134,9 +162,6 @@
     fetch(wd_hbm.at[0, :, mine_cols], wd.at[0])
     fetch(dd_hbm.at[:, mine_cols], dd.at[0])
     proj = jnp.dot(normed, wqkv[...], preferred_element_type=F32)
-    cosine, sine = trig[0], trig[1]
-    lane = lax.broadcasted_iota(jnp.int32, cosine.shape, 1)
-    upper = lane % HD >= HD // 2
 
     def rotated(x):
         swapped = jnp.where(upper, pltpu.roll(x, HD // 2, 1), pltpu.roll(x, 2 * HD - HD // 2, 1))
@@ -149,7 +174,7 @@
     key_new = rotated(proj[:, qw : qw + kw])
     value_new = proj[:, qw + kw :].astype(BF16).astype(F32)
 
-    pl.semaphore_wait(barrier, n)
+    pl.semaphore_wait(barrier, depth + plane - 1)
     their_cols = pl.ds(pl.multiple_of(other * half, 128), half)
     give_wd = pltpu.make_async_remote_copy(
         src_ref=wd_hbm.at[0, :, their_cols],
@@ -258,42 +283,61 @@
         buf[me, h, :, :half] = moe_in[:, h * half : (h + 1) * half]
         buf[me, h, :, half:] = extra_here
 
-    def gather_copy(d):
-        return pltpu.make_async_remote_copy(
-            src_ref=buf.at[me, core],
-            dst_ref=buf.at[me, core],
-            send_sem=gs.at[d],
-            recv_sem=gr.at[d],
-            device_id=(lax.rem(me + d, n), core),
-            device_id_type=MESH,
-        )
-
-    def gather_start(d, carry):
-        gather_copy(d).start()
-        return carry
-
-    lax.fori_loop(1, n, gather_start, 0)
-
-    def forward_copy(d):
-        source = lax.rem(me - d + n, n)
+    def gather_copy(source, target, send_sem):
         return pltpu.make_async_remote_copy(
             src_ref=buf.at[source, core],
             dst_ref=buf.at[source, core],
-            send_sem=fs.at[d],
-            recv_sem=fr.at[d],
+            send_sem=send_sem,
+            recv_sem=gr.at[source],
+            device_id=(target, core),
+            device_id_type=MESH,
+        )
+
+    def level_copy(d):
+        return gather_copy(me, level_mate(d), gz.at[d])
+
+    def plane_copy(d, k):
+        return gather_copy(level_mate(d), plane_mate(k), gs.at[d * plane + k])
+
+    def forward_copy(source):
+        return pltpu.make_async_remote_copy(
+            src_ref=buf.at[source, core],
+            dst_ref=buf.at[source, core],
+            send_sem=fs.at[source],
+            recv_sem=fr.at[source],
             device_id=partner,
             device_id_type=MESH,
         )
 
-    def forward(d, carry):
-        gather_copy(d).wait_recv()
-        forward_copy(d).start()
-        return carry
-
-    lax.fori_loop(1, n, forward, 0)
+    def share(d):
+        def start(k, carry):
+            plane_copy(d, k).start()
+            return carry
+
+        lax.fori_loop(1, plane, start, 0)
+
+    def arrive(source):
+        gather_copy(source, source, gz.at[0]).wait_recv()
+
+    for d in range(1, depth):
+        level_copy(d).start()
+    share(0)
+    for d in range(1, depth):
+        arrive(level_mate(d))
+        share(d)
+        forward_copy(level_mate(d)).start()
+    for d in range(depth):
+
+        def forward(k, carry, d=d):
+            source = lax.rem(level + d, depth) * plane + lax.rem(spot_here + k, plane)
+            arrive(source)
+            forward_copy(source).start()
+            return carry
+
+        lax.fori_loop(1, plane, forward, 0)
 
     def forward_done(d, carry):
-        forward_copy(d).wait_recv()
+        forward_copy(lax.rem(me + d, n)).wait_recv()
         return carry
 
     lax.fori_loop(1, n, forward_done, 0)
@@ -355,39 +399,71 @@
 
     lax.fori_loop(0, n // blocks, down, 0)
 
-    def scatter_copy(d):
-        target = lax.rem(me + d, n)
+    def near_copy(d, k):
         return pltpu.make_async_remote_copy(
-            src_ref=stage.at[target],
-            dst_ref=rbuf.at[d],
-            send_sem=rs.at[d],
-            recv_sem=rr.at[d],
-            device_id=(target, core),
+            src_ref=stage.at[lax.rem(level + d, depth) * plane + lax.rem(spot_here + k, plane)],
+            dst_ref=near.at[d * plane + k],
+            send_sem=rs.at[d * plane + k],
+            recv_sem=rr.at[d * plane + k],
+            device_id=(plane_mate(k), core),
             device_id_type=MESH,
         )
 
-    def scatter_start(d, carry):
-        scatter_copy(d).start()
+    def far_copy(d):
+        return pltpu.make_async_remote_copy(
+            src_ref=sums.at[d],
+            dst_ref=far.at[d],
+            send_sem=zs.at[d],
+            recv_sem=zr.at[d],
+            device_id=(level_mate(d), core),
+            device_id_type=MESH,
+        )
+
+    order = list(range(1, depth)) + [0]
+    for d in order:
+
+        def near_start(k, carry, d=d):
+            near_copy(d, k).start()
+            return carry
+
+        lax.fori_loop(1, plane, near_start, 0)
+    for d in order:
+        if d:
+            mine[...] = stage[level_mate(d)].astype(F32)
+        else:
+            mine[...] = resid[:, mine_cols] + stage[me].astype(F32)
+
+        def near_add(k, carry, d=d):
+            near_copy(d, k).wait_recv()
+            mine[...] += near[d * plane + k].astype(F32)
+            return carry
+
+        lax.fori_loop(1, plane, near_add, 0)
+        if d:
+            sums[d] = mine[...].astype(BF16)
+            far_copy(d).start()
+    for d in range(1, depth):
+        far_copy(d).wait_recv()
+        mine[...] += far[d].astype(F32)
+    out[...] = mine[...].astype(BF16)
+
+    for d in range(depth):
+
+        def drain(k, carry, d=d):
+            plane_copy(d, k).wait_send()
+            near_copy(d, k).wait_send()
+            return carry
+
+        lax.fori_loop(1, plane, drain, 0)
+        if d:
+            level_copy(d).wait_send()
+            far_copy(d).wait_send()
+
+    def forward_drain(d, carry):
+        forward_copy(lax.rem(me + d, n)).wait_send()
         return carry
 
-    lax.fori_loop(1, n, scatter_start, 0)
-    mine[...] = resid[:, mine_cols] + stage[me].astype(F32)
-
-    def collect(d, carry):
-        scatter_copy(d).wait_recv()
-        mine[...] += rbuf[d].astype(F32)
-        return carry
-
-    lax.fori_loop(1, n, collect, 0)
-    out[...] = mine[...].astype(BF16)
-
-    def drain(d, carry):
-        gather_copy(d).wait_send()
-        forward_copy(d).wait_send()
-        scatter_copy(d).wait_send()
-        return carry
-
-    lax.fori_loop(1, n, drain, 0)
+    lax.fori_loop(1, n, forward_drain, 0)
     swap.wait_send()
     give_wd.wait_send()
     give_dd.wait_send()
@@ -425,12 +501,8 @@
     span = cache_keys.shape[1]
     experts = w_router.shape[1]
     group = lambdas.shape[0]
-    inverse = 10000.0 ** (-jnp.arange(HD // 2, dtype=F32) / (HD // 2))
-    angle = lengths.astype(F32)[:, None] * inverse
-    cosine, sine = jnp.cos(angle), jnp.sin(angle)
-    trig = jnp.stack(
-        [jnp.concatenate([cosine] * 4, 1), jnp.concatenate([-sine, sine, -sine, sine], 1)]
-    )
+    inverse = 10000.0 ** (-np.arange(HD // 2, dtype=np.float32) / np.float32(HD // 2))
+    inverse = jnp.asarray(np.tile(inverse.astype(np.float32), 4)[None])
     w_small = jnp.concatenate([w_router, w_group, w_blend[:, None]], 1)
     w_small = jnp.pad(w_small, ((0, 0), (0, -w_small.shape[1] % 128)))
     lanes = w_small.shape[1]
@@ -471,9 +543,12 @@
             pltpu.VMEM((n, seqs, half), BF16),
             pltpu.VMEM((seqs, half), F32),
             pltpu.VMEM((n, seqs, half), BF16),
+            pltpu.VMEM((4, seqs, half), BF16),
+            pltpu.VMEM((4, seqs, half), BF16),
             dma((18,)),
             dma((1,)),
             dma((1,)),
+            dma((4,)),
             dma((n,)),
             dma((n,)),
             dma((n,)),
@@ -484,6 +559,8 @@
             dma((2,)),
             dma((n,)),
             dma((n,)),
+            dma((4,)),
+            dma((4,)),
         ],
         compiler_params=pltpu.CompilerParams(collective_id=0, has_side_effects=True),
         name="layer",
@@ -491,7 +568,7 @@
         lengths,
         lambdas,
         tokens,
-        trig,
+        inverse,
         gain_first.reshape(1, -1),
         head_gain,
         gain_second.reshape(1, -1),

time: 51.6 us -> 45.8 us (0.89)
  the two profiles are of different devices: /device:TPU:28 before, /device:TPU:0 now
where the time goes in v2:
time: 45.8 us; the launch traced here: 45.5 us
  Pallas kernels  40 us (87%)
  local copies, waits for them, and re-layouts  4.62 us (10%)
  other arithmetic  0.88 us (2%)
    pallas_call x1, Pallas kernels, local(): pl.pallas_call(functools.partial(layer_kernel, n, experts), out_shape=jax...  40 us
    unnamed x2, local copies, waits for them, and re-layouts  2.73 us

profile of v2, /device:TPU:0, one launch (start us, length us, event | category | flops | bytes accessed | tf_op | source)
XLA Modules:
  0.0 45.5 jit_solution(7303811475758459451)
XLA Ops:
  0.0 0.7 %broadcast_in_dim.3 = bf16[2048,1]{0,1:T(2,128)(2,1)S(1)} reshape(bf16[2048]{0:T(1024)(128)(2,1)} %param.37) | data formatting | bytes 8192 | tf_op jit(solution)/shard_map/broadcast_in_dim | solution.py:506
  0.7 0.9 %pad_maximum_fusion = bf16[2048,21]{0,1:T(8,128)(2,1)S(1)} fusion(bf16[2048,1]{0,1:T(2,128)(2,1)S(1)} %broadcast_in_dim.3, bf16[2048,4]{0,1:T(4,128)(2,1)} %param.35, bf16[2048,16]{0,1:T(8,128)(2,1)} %param.36), kind=kLoop, calls=%fused_computation | loop fusion | flops 258048 | bytes 172032 | tf_op jit(solution)/shard_map/concatenate | solution.py:506
  1.6 0.3 copy.31
  1.9 0.9 %pad.4.w_small = bf16[2048,128]{1,0:T(8,128)(2,1)} pad(bf16[2048,21]{1,0:T(8,128)(2,1)S(1)} %copy.31, bf16[]{:T(256)} %constant.4.clone.1), padding=0_0x0_107 | pad | bytes 610306 | tf_op jit(solution)/shard_map/jit(_pad)/pad | solution.py:507
  2.8 1.4 %copy.32.routes = s32[16,4]{1,0:T(8,128)} copy(s32[16,4]{0,1:T(4,128)} %param.38) | data formatting | bytes 512 | tf_op args[15]
  4.1 40.0 %layer.1 = bf16[16,1024]{1,0:T(8,128)(2,1)} custom-call(s32[16]{0:T(128)} %lengths.1, f32[4]{0:T(128)} %lambdas.1, bf16[16,2048]{1,0:T(8,128)(2,1)} %tokens.1, f32[1,128]{1,0:T(1,128)} %constant.5.clone.inverse, f32[1,2048]{1,0:T(1,128)} %bitcast.2, f32[4,128]{1,0:T(4,128)} %head_gain.1, f32[1,2048]{1,0:T(1,128)} %bitcast.3, s32[16,4]{1,0:T(8,128)} %copy.32.routes, ...), custom_call_target="tpu_custom_call" | custom-call | tf_op jit(solution)/shard_map/layer/pallas_call | solution.py:521
  44.1 1.4 %copy.34 = bf16[16,1024]{1,0:T(8,128)(2,1)} copy(bf16[16,1024]{1,0:T(8,128)(2,1)} %layer.1) | data formatting | bytes 65536
